TPU v7x, 32 devices: a whole 2x2x4 slice. The times are simulated.
32 devices in a mesh: sp: 4 (over y, core), dp: 8 (over z, x).
Axes of the slice: x: 2, y: 2, z: 4, core: 2. Of those that a mesh axis runs over, the one named last changes fastest.
Arguments:
- standardized_block_source: bfloat16 [16, 256, 2064], P('dp', 'sp'), may hold values from -6 to 6
- forgetting_narrowing_matrix: bfloat16 [2064, 32], P('dp'), may hold values from -0.125 to 0.125
- forgetting_widening_matrix: bfloat16 [32, 1024], replicated, may hold values from -1 to 1
- forgetting_offset_vector: float32 [1024], replicated, may hold values from -1.5 to 6.5
- probe_vectors: bfloat16 [128, 256, 128], P(('dp', 'sp')), may hold values from -6 to 6
- address_vectors: bfloat16 [128, 256, 128], P(('dp', 'sp')), may hold values from -6 to 6
- payload_vectors: bfloat16 [128, 256, 256], P(('dp', 'sp')), may hold values from -6 to 6
- extra_channel_forgetting: float32 [128, 256], P(('dp', 'sp')), may hold values from -2.1 to 0
- blender_result_adjoint: bfloat16 [16, 256, 2048], P('dp', 'sp'), may hold values from -0.29882812 to 0.29882812
Outputs:
- grad_queries: bfloat16 [16, 256, 1024], P('dp', 'sp')
- grad_keys: bfloat16 [16, 256, 1024], P('dp', 'sp')
- grad_values: bfloat16 [16, 256, 2048], P('dp', 'sp')
- grad_input: bfloat16 [16, 256, 2064], P('dp', 'sp')
- grad_gate_down: float32 [2064, 32], P('dp')
- grad_gate_up: float32 [32, 1024], replicated
- grad_gate_bias: float32 [1024], replicated
All inputs are finite; a program needn't handle non-finite values.
Results may differ from a plain program's by a relative error of at most 0.0069.
Values may be sent and summed in bfloat16 or wider, within the bound.
A program may use at most 64 MiB of HBM per device.

v0:
```python
import jax
import jax.numpy as jnp
from jax import lax
from jax.sharding import PartitionSpec as P

HEADS = 8
ADDRESS_WIDTH = 128
PAYLOAD_WIDTH = 256
BLOCK = 64


retention_smoothing = 16.0


def head_forward(
    stream_probe_entries, stream_address_entries, stream_payload_entries, retention_coefficient
):
    length, key_width = stream_probe_entries.shape
    value_width = stream_payload_entries.shape[1]
    blocks = length // BLOCK
    middle = BLOCK // 2
    scaled = stream_probe_entries * key_width ** (-0.5)
    causal = jnp.tril(jnp.ones((BLOCK, BLOCK), dtype=bool))
    highest = lax.Precision.HIGHEST

    def advance(memory, pieces):
        query_block, key_block, value_block, decay_sums = pieces
        centre = decay_sums[middle]
        lifted_query = query_block * jnp.exp(decay_sums - centre[None, :])
        lowered_key = key_block * jnp.exp(centre[None, :] - decay_sums)
        raw_scores = jnp.dot(lifted_query, lowered_key.T, precision=highest)
        scores = jnp.where(causal, raw_scores, 0.0)
        within = jnp.dot(scores, value_block, precision=highest)
        carried = jnp.dot(query_block * jnp.exp(decay_sums), memory, precision=highest)
        ending = decay_sums[-1]
        fading = key_block * jnp.exp(ending[None, :] - decay_sums)
        memory = memory * jnp.exp(ending)[:, None] + jnp.dot(
            fading.T, value_block, precision=highest
        )
        return (memory, within + carried)

    def blocked(tensor):
        return tensor.reshape(blocks, BLOCK, tensor.shape[1])

    initial = jnp.zeros((key_width, value_width), jnp.float32)
    decay_sums = jnp.cumsum(blocked(retention_coefficient), axis=1)
    _, outputs = lax.scan(
        jax.checkpoint(advance),
        initial,
        (
            blocked(scaled),
            blocked(stream_address_entries),
            blocked(stream_payload_entries),
            decay_sums,
        ),
    )
    return outputs.reshape(length, value_width)


def stream_sensitivities(
    stream_probe_entries,
    stream_address_entries,
    stream_payload_entries,
    forgetting_logit_values,
    surplus_retention_loss,
    result_adjoint,
):

    def forward(query_in, key_in, value_in, retention_basis_components):
        retention_coefficient = (
            jax.nn.log_sigmoid(retention_basis_components) / retention_smoothing
            + surplus_retention_loss[:, None]
        )
        return head_forward(query_in, key_in, value_in, retention_coefficient)

    _, pullback = jax.vjp(
        forward,
        stream_probe_entries.astype(jnp.float32),
        stream_address_entries.astype(jnp.float32),
        stream_payload_entries.astype(jnp.float32),
        forgetting_logit_values,
    )
    query_grad, key_grad, value_grad, gate_grad = pullback(result_adjoint.astype(jnp.float32))
    return (
        query_grad.astype(jnp.bfloat16),
        key_grad.astype(jnp.bfloat16),
        value_grad.astype(jnp.bfloat16),
        gate_grad.astype(jnp.bfloat16),
    )


def on_device(
    standardized_block_source,
    forgetting_narrowing_matrix,
    forgetting_widening_matrix,
    forgetting_offset_vector,
    probe_vectors,
    address_vectors,
    payload_vectors,
    extra_channel_forgetting,
    blender_result_adjoint,
):
    seqs, local_len, model_width = standardized_block_source.shape
    tokens_dev = seqs * local_len
    contract = (((0,), (0,)), ((), ()))
    flat_input = standardized_block_source.reshape(tokens_dev, model_width)
    down_whole = lax.all_gather(forgetting_narrowing_matrix, "dp", axis=0, tiled=True)
    low_rank = jnp.dot(flat_input, down_whole, preferred_element_type=jnp.float32).astype(
        jnp.bfloat16
    )
    logit_by_position = (
        jnp.dot(low_rank, forgetting_widening_matrix, preferred_element_type=jnp.float32)
        + forgetting_offset_vector
    )
    pre_items = (
        logit_by_position.reshape(seqs, local_len, HEADS, ADDRESS_WIDTH)
        .transpose(0, 2, 1, 3)
        .reshape(seqs * HEADS, local_len, ADDRESS_WIDTH)
    )
    logit_by_stream = lax.all_to_all(pre_items, "sp", split_axis=0, concat_axis=1, tiled=True)
    cot_items = (
        blender_result_adjoint.reshape(seqs, local_len, HEADS, PAYLOAD_WIDTH)
        .transpose(0, 2, 1, 3)
        .reshape(seqs * HEADS, local_len, PAYLOAD_WIDTH)
    )
    adjoint_split_by_stream = lax.all_to_all(
        cot_items, "sp", split_axis=0, concat_axis=1, tiled=True
    )
    query_grad, key_grad, value_grad, gate_grad = jax.vmap(stream_sensitivities)(
        probe_vectors,
        address_vectors,
        payload_vectors,
        logit_by_stream,
        extra_channel_forgetting,
        adjoint_split_by_stream,
    )
    returned = (
        lax.all_to_all(query_grad, "sp", split_axis=1, concat_axis=0, tiled=True),
        lax.all_to_all(key_grad, "sp", split_axis=1, concat_axis=0, tiled=True),
        lax.all_to_all(value_grad, "sp", split_axis=1, concat_axis=0, tiled=True),
        lax.all_to_all(gate_grad, "sp", split_axis=1, concat_axis=0, tiled=True),
    )

    def to_tokens(tensor):
        columns = tensor.shape[2]
        return (
            tensor.reshape(seqs, HEADS, local_len, columns)
            .transpose(0, 2, 1, 3)
            .reshape(seqs, local_len, HEADS * columns)
        )

    gate_tokens = to_tokens(returned[3]).reshape(tokens_dev, HEADS * ADDRESS_WIDTH)
    low_grad = jnp.dot(
        gate_tokens, forgetting_widening_matrix.T, preferred_element_type=jnp.float32
    ).astype(jnp.bfloat16)
    incoming_sensitivity = jnp.dot(
        low_grad, down_whole.T, preferred_element_type=jnp.float32
    ).astype(jnp.bfloat16)
    up_term = lax.dot_general(low_rank, gate_tokens, contract, preferred_element_type=jnp.float32)
    bias_term = jnp.sum(gate_tokens.astype(jnp.float32), axis=0)
    partition_lines_count = forgetting_narrowing_matrix.shape[0]
    whole_term = lax.dot_general(flat_input, low_grad, contract, preferred_element_type=jnp.float32)
    combined_contraction, up_grad, bias_grad = lax.psum(
        (whole_term, up_term, bias_term), ("sp", "dp")
    )
    down_grad = lax.dynamic_slice_in_dim(
        combined_contraction, lax.axis_index("dp") * partition_lines_count, partition_lines_count, 0
    )
    return (
        to_tokens(returned[0]),
        to_tokens(returned[1]),
        to_tokens(returned[2]),
        incoming_sensitivity.reshape(seqs, local_len, model_width),
        down_grad,
        up_grad,
        bias_grad,
    )


def solution(mesh):
    placed = (
        P("dp", "sp", None),
        P("dp", None),
        P(),
        P(),
        P(("dp", "sp"), None, None),
        P(("dp", "sp"), None, None),
        P(("dp", "sp"), None, None),
        P(("dp", "sp"), None),
        P("dp", "sp", None),
    )
    return jax.shard_map(
        on_device,
        mesh=mesh,
        in_specs=placed,
        out_specs=(
            P("dp", "sp", None),
            P("dp", "sp", None),
            P("dp", "sp", None),
            P("dp", "sp", None),
            P("dp", None),
            P(),
            P(),
        ),
        check_vma=False,
    )
```

profile of v0, /device:TPU:29, one launch (start us, length us, event | category | flops | bytes accessed | tf_op | source)
XLA Modules:
  0.0 300.1 jit_solution(9182041822408000112)
XLA Ops:
  7.2 22.2 %all-gather = bf16[8,258,32]{1,2,0:T(8,128)(2,1)S(1)} all-gather(bf16[1,258,32]{1,2,0:T(8,128)(2,1)} %bitcast.296), channel_id=1, replica_groups=mesh['sp'=4,'dp'=8] {'dp'}, dimensions={0}, use_global_device_ids=true | all-gather | bytes 148608 | tf_op jit(solution)/shard_map/all_gather | solution.py:107
  30.0 1.1 fusion.27
  32.1 10.3 %all-to-all-start = ((f32[16,64,128]{2,1,0:T(8,128)}), f32[16,64,128]{2,1,0:T(8,128)S(1)}, u32[]{:S(2)}, u32[]{:S(2)}) async-start(f32[16,64,128]{2,1,0:T(8,128)} %bitcast.3), calls=%async_computation | async-start | bytes 1048576 | tf_op jit(solution)/shard_map/all_to_all | solution.py:120
  42.5 1.2 copy.147
  50.3 5.8 %all-to-all-start.1 = ((bf16[16,64,256]{2,1,0:T(8,128)(2,1)}), bf16[16,64,256]{2,1,0:T(8,128)(2,1)}, u32[]{:S(2)}, u32[]{:S(2)}) async-start(bf16[16,64,256]{2,1,0:T(8,128)(2,1)} %bitcast.16), calls=%async_computation.1 | async-start | bytes 1048576 | tf_op jit(solution)/shard_map/all_to_all | solution.py:126
  57.5 1.2 reduce_window_sum.22
  59.8 10.3 %while.36 = (s32[]{:T(128)}, f32[4,128,256]{2,1,0:T(8,128)S(1)}, f32[4,4,128,256]{3,2,1,0:T(8,128)}, f32[4,4,64,128]{3,2,1,0:T(8,128)S(1)}, f32[4,4,64,128]{3,2,...) while((s32[]{:T(128)}, f32[4,128,256]{2,1,0:T(8,128)S(1)}, ...), condition=%wide.region_2.3_spmd.clone, body=%wide.region_1.2_spmd.clone.sunk | while | flops 101253120 | bytes 2897508 | solution.py:47
  60.7 1.6 convolution_add_fusion.6
  63.3 1.6 convolution_add_fusion.6
  65.9 1.6 convolution_add_fusion.6
  68.4 1.6 convolution_add_fusion.6
  70.9 2.1 convert.7
  75.6 38.5 %while.37 = (s32[]{:T(128)}, f32[4,128,256]{2,1,0:T(8,128)S(1)}, f32[4,4,64,128]{3,2,0,1:T(8,128)}, bf16[4,4,64,128]{3,2,0,1:T(8,128)(2,1)}, bf16[4,4,64,256]{3,...) while((s32[]{:T(128)}, f32[4,128,256]{2,1,0:T(8,128)S(1)}, ...), condition=%wide.region_8.9_spmd.clone, body=%wide.region_3.8_spmd.clone.sunk | while | flops 581210112 | bytes 23470384 | solution.py:47
  75.6 1.3 dynamic-slice_bitcast_fusion.17
  81.0 1.1 bitcast_dynamic-update-slice_fusion.8
  85.3 1.3 dynamic-slice_bitcast_fusion.17
  94.9 1.3 dynamic-slice_bitcast_fusion.17
  104.5 1.3 dynamic-slice_bitcast_fusion.17
  109.9 1.1 bitcast_dynamic-update-slice_fusion.8
  114.2 5.7 %reduce_window_sum.23 = f32[4,4,64,128]{3,2,1,0:T(8,128)S(1)} reduce-window(f32[4,4,64,128]{3,2,1,0:T(8,128)} %get-tuple-element.309, f32[]{:T(128)} %constant.99.clone.1), window={size=1x1x64x1 pad=0_0x0_0x0_63x0_0}, to_apply=%region_9.10 | reduce-window | flops 8257536 | bytes 1048580 | tf_op jit(solution)/shard_map/vmap(transpose(jvp(jit(cumsum))))/reduce_window_sum | solution.py:46
  121.4 3.6 %all-to-all-start.5 = ((bf16[4,256,128]{2,0,1:T(4,128)(2,1)}), bf16[4,256,128]{2,0,1:T(4,128)(2,1)S(1)}, u32[]{:S(2)}, u32[]{:S(2)}) async-start(bf16[4,256,128]{2,0,1:T(4,128)(2,1)} %copy.126), calls=%async_computation.5 | async-start | bytes 524288 | tf_op jit(solution)/shard_map/all_to_all | solution.py:141
  125.9 1.9 copy.116
  127.8 1.2 copy.121
  129.0 5.3 %all-to-all-start.2 = ((bf16[4,256,128]{2,0,1:T(4,128)(2,1)}), bf16[4,256,128]{2,0,1:T(4,128)(2,1)S(1)}, u32[]{:S(2)}, u32[]{:S(2)}) async-start(bf16[4,256,128]{2,0,1:T(4,128)(2,1)} %copy.111), calls=%async_computation.2 | async-start | bytes 524288 | tf_op jit(solution)/shard_map/all_to_all | solution.py:138
  135.7 2.8 all-to-all-done.2
  138.5 5.2 %all-to-all-start.3 = ((bf16[4,256,128]{2,0,1:T(4,128)(2,1)}), bf16[4,256,128]{2,0,1:T(4,128)(2,1)S(1)}, u32[]{:S(2)}, u32[]{:S(2)}) async-start(bf16[4,256,128]{2,0,1:T(4,128)(2,1)} %copy.116), calls=%async_computation.3 | async-start | bytes 524288 | tf_op jit(solution)/shard_map/all_to_all | solution.py:139
  144.0 3.8 %all-to-all-done.3 = bf16[4,256,128]{2,0,1:T(4,128)(2,1)S(1)} async-done(((bf16[4,256,128]{2,0,1:T(4,128)(2,1)}), bf16[4,256,128]{2,0,1:T(4,128)(2,1)S(1)}, u32[]{:S(2)}, u32[]{:S(2)}) %all-to-all-start.3) | async-done | bytes 262176 | tf_op jit(solution)/shard_map/all_to_all | solution.py:139
  147.8 5.3 %all-to-all-start.4 = ((bf16[4,256,256]{2,0,1:T(4,128)(2,1)}), bf16[4,256,256]{2,0,1:T(4,128)(2,1)S(1)}, u32[]{:S(2)}, u32[]{:S(2)}) async-start(bf16[4,256,256]{2,0,1:T(4,128)(2,1)} %copy.121), calls=%async_computation.4 | async-start | bytes 1048576 | tf_op jit(solution)/shard_map/all_to_all | solution.py:140
  155.2 40.0 %psum.23 = f32[1024]{0:T(1024)} all-reduce(f32[1024]{0:T(1024)S(1)} %bitcast.297), channel_id=1, replica_groups=mesh['sp'=4,'dp'=8] {'sp','dp'}, use_global_device_ids=true, to_apply=%region_13.14 | all-reduce | flops 1024 | bytes 8192 | tf_op jit(solution)/shard_map/psum | solution.py:163
  197.1 93.1 %all-reduce.5.cloned.1.call-done = (f32[2064,32]{0,1:T(8,128)}, f32[32,1024]{1,0:T(8,128)}) async-done(((f32[2064,32]{0,1:T(8,128)}, f32[32,1024]{1,0:T(8,128)}), (f32[2064,32]{0,1:T(8,128)}, f32[32,1024]{1,0:T(8,128)})) %all-reduce.5.cloned.1.call-update) | async-done | bytes 395280 | tf_op jit(solution)/shard_map/psum | solution.py:163
  290.1 1.5 constant_dynamic-slice_fusion
  291.7 1.6 copy.194
  (207 shorter events, 56.3 us)
Async XLA Ops:
  7.2 22.5 %copy-start = (bf16[2,64,2064]{2,1,0:T(8,128)(2,1)S(1)}, bf16[2,64,2064]{2,1,0:T(8,128)(2,1)}, u32[]{:S(2)}) copy-start(bf16[2,64,2064]{2,1,0:T(8,128)(2,1)} %param.13) | copy-start | bytes 1585156
  29.7 12.7 %copy-start.11 = (bf16[4,256,256]{2,1,0:T(8,128)(2,1)S(1)}, bf16[4,256,256]{2,1,0:T(8,128)(2,1)}, u32[]{:S(2)}) copy-start(bf16[4,256,256]{2,1,0:T(8,128)(2,1)} %param.19) | copy-start | bytes 1572868
  32.1 17.4 %all-to-all-start = ((f32[16,64,128]{2,1,0:T(8,128)}), f32[16,64,128]{2,1,0:T(8,128)S(1)}, u32[]{:S(2)}, u32[]{:S(2)}) async-start(f32[16,64,128]{2,1,0:T(8,128)} %bitcast.3), calls=%async_computation | async-start | bytes 1048576 | tf_op jit(solution)/shard_map/all_to_all | solution.py:120
  42.4 2.1 copy-start.12
  42.4 3.0 copy-start.15
  45.4 1.1 copy-start.10
  45.4 1.6 copy-start.6
  46.6 2.1 copy-start.13
  50.3 20.6 %all-to-all-start.1 = ((bf16[16,64,256]{2,1,0:T(8,128)(2,1)}), bf16[16,64,256]{2,1,0:T(8,128)(2,1)}, u32[]{:S(2)}, u32[]{:S(2)}) async-start(bf16[16,64,256]{2,1,0:T(8,128)(2,1)} %bitcast.16), calls=%async_computation.1 | async-start | bytes 1048576 | tf_op jit(solution)/shard_map/all_to_all | solution.py:126
  75.6 1.3 copy-start.1
  82.2 1.8 copy-start.7
  83.2 2.1 copy-start.2
  84.5 0.8 copy-start.8
  85.3 1.3 copy-start.1
  91.9 1.8 copy-start.7
  92.8 2.1 copy-start.2
  94.9 1.3 copy-start.1
  101.5 1.8 copy-start.7
  102.5 2.1 copy-start.2
  103.7 0.8 copy-start.8
  104.5 1.3 copy-start.1
  111.1 1.8 copy-start.7
  112.1 2.1 copy-start.2
  114.2 5.8 %copy-start.4 = (f32[4,4,64,128]{3,2,0,1:T(8,128)S(1)}, f32[4,4,64,128]{3,2,0,1:T(8,128)}, u32[]{:S(2)}) copy-start(f32[4,4,64,128]{3,2,0,1:T(8,128)} %copy.101) | copy-start | bytes 1572868
  119.8 5.1 %copy-start.3 = (f32[4,4,64,128]{3,2,0,1:T(8,128)S(1)}, f32[4,4,64,128]{3,2,0,1:T(8,128)}, u32[]{:S(2)}) copy-start(f32[4,4,64,128]{3,2,0,1:T(8,128)} %get-tuple-element.306) | copy-start | bytes 1572868
  120.0 7.8 %copy-start.9 = (bf16[4,4,64,256]{3,2,0,1:T(8,128)(2,1)S(1)}, bf16[4,4,64,256]{3,2,0,1:T(8,128)(2,1)}, u32[]{:S(2)}) copy-start(bf16[4,4,64,256]{3,2,0,1:T(8,128)(2,1)} %get-tuple-element.308) | copy-start | bytes 1572868
  121.4 7.7 %all-to-all-start.5 = ((bf16[4,256,128]{2,0,1:T(4,128)(2,1)}), bf16[4,256,128]{2,0,1:T(4,128)(2,1)S(1)}, u32[]{:S(2)}, u32[]{:S(2)}) async-start(bf16[4,256,128]{2,0,1:T(4,128)(2,1)} %copy.126), calls=%async_computation.5 | async-start | bytes 524288 | tf_op jit(solution)/shard_map/all_to_all | solution.py:141
  125.0 9.5 %copy-start.14 = (bf16[32,1024]{1,0:T(8,128)(2,1)S(1)}, bf16[32,1024]{1,0:T(8,128)(2,1)}, u32[]{:S(2)}) copy-start(bf16[32,1024]{1,0:T(8,128)(2,1)} %param.15) | copy-start | bytes 196612
  129.0 9.4 %all-to-all-start.2 = ((bf16[4,256,128]{2,0,1:T(4,128)(2,1)}), bf16[4,256,128]{2,0,1:T(4,128)(2,1)S(1)}, u32[]{:S(2)}, u32[]{:S(2)}) async-start(bf16[4,256,128]{2,0,1:T(4,128)(2,1)} %copy.111), calls=%async_computation.2 | async-start | bytes 524288 | tf_op jit(solution)/shard_map/all_to_all | solution.py:138
  138.5 9.4 %all-to-all-start.3 = ((bf16[4,256,128]{2,0,1:T(4,128)(2,1)}), bf16[4,256,128]{2,0,1:T(4,128)(2,1)S(1)}, u32[]{:S(2)}, u32[]{:S(2)}) async-start(bf16[4,256,128]{2,0,1:T(4,128)(2,1)} %copy.116), calls=%async_computation.3 | async-start | bytes 524288 | tf_op jit(solution)/shard_map/all_to_all | solution.py:139
  147.8 48.3 %all-to-all-start.4 = ((bf16[4,256,256]{2,0,1:T(4,128)(2,1)}), bf16[4,256,256]{2,0,1:T(4,128)(2,1)S(1)}, u32[]{:S(2)}, u32[]{:S(2)}) async-start(bf16[4,256,256]{2,0,1:T(4,128)(2,1)} %copy.121), calls=%async_computation.4 | async-start | bytes 1048576 | tf_op jit(solution)/shard_map/all_to_all | solution.py:140
  153.1 137.0 %all-reduce.5.cloned.1.call-start = ((), (), s32[]{:S(2)}) async-start(), calls=%async_computation.6 | async-start | bytes 819200 | tf_op jit(solution)/shard_map/psum | solution.py:163
  (3 other events, 2.4 us)
Sparse Core Ops, SparseCore 0:
  159.9 130.2 all-reduce.4
where the time goes:
time: 304 us; the launch traced here: 300 us
  waiting for transfers between devices  99.7 us (33%)
  blocking collectives  62.2 us (20%)
  local copies, waits for them, and re-layouts  36.1 us (12%)
  starting transfers between devices  35.4 us (12%)
  matrix products  30 us (10%)
  other arithmetic  21.5 us (7%)
  between operations  14.3 us (5%)
    psum x1, waiting for transfers between devices, on_device(): lax.psum((whole_term, up_term, bias_term), ('sp', 'dp'))  93.1 us
    psum x1, blocking collectives, on_device(): lax.psum((whole_term, up_term, bias_term), ('sp', 'dp'))  40 us
    all_gather x1, blocking collectives, on_device(): lax.all_gather(forgetting_narrowing_matrix, 'dp', axis=0, tiled=True)  22.2 us
    squeeze x20, local copies, waits for them, and re-layouts, head_forward(): lax.scan(jax.checkpoint(advance), initial, (blocked(scaled), blocked(stre...  13.2 us
    dot_general x12, matrix products, advance(): jnp.dot(fading.T, value_block, precision=highest)  11 us
    all_to_all x1, starting transfers between devices, on_device(): lax.all_to_all(pre_items, 'sp', split_axis=0, concat_axis=1, tiled=True)  10.3 us
    another operation x2, other arithmetic, head_forward(): decay_sums = jnp.cumsum(blocked(retention_coefficient), axis=1)  6.91 us
    dot_general x12, matrix products, advance(): raw_scores = jnp.dot(lifted_query, lowered_key.T, precision=highest)  6.88 us
  transfers between devices with their start and end apart: 7, of which 3 were waited for; matrix products, arithmetic and copies ran while one was open for 10% of the time, Pallas kernels for 0%

commit v1 on v0

v1 whole, which is shorter than its diff:
```python
import functools

import jax
import jax.numpy as jnp
from jax import lax
from jax.experimental import pallas as pl
from jax.experimental.pallas import tpu as pltpu
from jax.sharding import PartitionSpec as P

HEADS = 8
KW = 128
VW = 256
BLOCK = 64
SMOOTH = 16.0
MESH = pl.DeviceIdType.MESH
F32 = jnp.float32
BF = jnp.bfloat16
NN = (((1,), (0,)), ((), ()))
NT = (((1,), (1,)), ((), ()))
TN = (((0,), (0,)), ((), ()))


def dot(a, b, dims=NN):
    return lax.dot_general(a, b, dims, preferred_element_type=F32)


def split(x, parts):
    out = []
    for _ in range(parts - 1):
        hi = x.astype(BF)
        out.append(hi)
        x = x - hi.astype(F32)
    out.append(x.astype(BF))
    return out


def kernel(
    n_sp, n_dp, seqs, rows,
    xp_ref, dt_ref, up_ref, offs_ref, q_ref, k_ref, v_ref, extra_ref, adj_ref,
    gqkv_ref, gi_ref, gd_ref, gu_ref,
    down_all, low_all, adj_in, gbuf, state, states, dstate, bsum, slope, gpre,
    glp, glp_in, gdp, gd_in, gd_sum, ub, ub_in, ub_sum,
    s_down, r_down, s_adj, r_adj, s_low, r_low, s_g, r_g, s_gl, r_gl,
    s_gd, r_gd, s_gs, r_gs, s_ub, r_ub, s_us, r_us,
):
    sp, dp = lax.axis_index("sp"), lax.axis_index("dp")
    n_all = n_sp * n_dp
    me = dp * n_sp + sp
    rank = dt_ref.shape[0]
    nj = rank // 8
    blocks = n_sp
    seq_of_me = (sp * rows) // HEADS
    head0 = lax.rem(sp * rows, HEADS)
    scale = KW ** (-0.5)

    def remote(src, dst, ss, rs, to_sp, to_dp):
        return pltpu.make_async_remote_copy(
            src_ref=src, dst_ref=dst, send_sem=ss, recv_sem=rs,
            device_id={"sp": to_sp, "dp": to_dp}, device_id_type=MESH,
        )

    barrier = pltpu.get_barrier_semaphore()

    @pl.loop(1, n_all)
    def _(d):
        other = lax.rem(me + d, n_all)
        pl.semaphore_signal(
            barrier, inc=1,
            device_id={"sp": lax.rem(other, n_sp), "dp": other // n_sp}, device_id_type=MESH,
        )

    pl.semaphore_wait(barrier, n_all - 1)

    def down_copy(d):
        to = lax.rem(dp + d, n_dp)
        return remote(dt_ref, down_all.at[dp], s_down.at[d], r_down.at[dp], sp, to)

    @pl.loop(1, n_dp)
    def _(d):
        down_copy(d).start()

    def adj_copy(d):
        to = lax.rem(sp + d, n_sp)
        return remote(
            adj_ref.at[pl.ds(to * rows, rows)], adj_in.at[sp], s_adj.at[d], r_adj.at[sp], to, dp
        )

    for d in range(1, n_sp):
        adj_copy(d).start()

    down_all[dp] = dt_ref[...]
    adj_in[sp] = adj_ref[pl.ds(sp * rows, rows)]

    tokens = seqs * BLOCK

    def wait_recv(dst, sem):
        remote(dst, dst, sem, sem, sp, dp).wait_recv()

    def low_step(d, acc):
        i = lax.rem(dp + d, n_dp)

        @pl.when(d > 0)
        def _():
            wait_recv(down_all.at[i], r_down.at[i])

        return acc + dot(xp_ref[i], down_all[i], NT)

    low = lax.fori_loop(0, n_dp, low_step, jnp.zeros((tokens, rank), F32)).astype(BF)
    low_all[sp] = low

    def low_copy(d):
        to = lax.rem(sp + d, n_sp)
        return remote(low_all.at[sp], low_all.at[sp], s_low.at[d], r_low.at[sp], to, dp)

    for d in range(1, n_sp):
        low_copy(d).start()

    r_i = lax.broadcasted_iota(jnp.int32, (BLOCK, BLOCK), 0)
    c_i = lax.broadcasted_iota(jnp.int32, (BLOCK, BLOCK), 1)
    causal = r_i >= c_i
    tril = causal.astype(F32).astype(BF)
    triu = (c_i >= r_i).astype(F32).astype(BF)
    below = (r_i > c_i).astype(F32).astype(BF)
    sum_mat = jnp.concatenate([tril] * 3, axis=1)
    grad_mat = jnp.concatenate([triu, triu, below, below], axis=1)
    up_mine = up_ref[:, pl.ds(pl.multiple_of(head0 * KW, KW), rows * KW)]
    offs_mine = offs_ref[:, pl.ds(pl.multiple_of(head0 * KW, KW), rows * KW)]
    state[...] = jnp.zeros_like(state)
    dstate[...] = jnp.zeros_like(dstate)

    @pl.loop(0, blocks)
    def _(t):
        @pl.when(t != sp)
        def _():
            wait_recv(low_all.at[t], r_low.at[t])

        low_t = low_all[t, pl.ds(pl.multiple_of(seq_of_me * BLOCK, BLOCK), BLOCK), :]
        pre = dot(low_t, up_mine) + offs_mine
        at = pl.ds(pl.multiple_of(t * BLOCK, BLOCK), BLOCK)
        e = jnp.exp(-jnp.abs(pre))
        logsig = jnp.minimum(pre, 0.0) - jnp.log1p(e)
        slope[t] = jnp.where(pre >= 0, e, 1.0) / (1.0 + e) * (1.0 / SMOOTH)
        ld = logsig * (1.0 / SMOOTH) + jnp.concatenate(
            [jnp.broadcast_to(extra_ref[i, at, :], (BLOCK, KW)) for i in range(rows)], axis=1
        )
        sums = dot(sum_mat, jnp.concatenate(split(ld, 3), axis=0))
        bsum[t] = sums
        for i in range(rows):
            b = sums[:, i * KW : (i + 1) * KW]
            last = b[BLOCK - 1 : BLOCK, :]
            kh = (k_ref[i, at, :].astype(F32) * jnp.exp(last - b)).astype(BF)
            s = state[i]
            states[t, i] = s.astype(BF)
            state[i] = s * jnp.exp(last) + dot(v_ref[i, at, :], kh, TN)

    def g_copy(t):
        return remote(
            gbuf.at[t], gqkv_ref.at[pl.ds(sp * rows, rows)], s_g.at[t], r_g.at[sp], t, dp
        )

    def gl_copy(t):
        return remote(glp.at[t], glp_in.at[sp], s_gl.at[t], r_gl.at[sp], t, dp)

    middle = BLOCK // 2

    @pl.loop(0, blocks)
    def _(step):
        t = blocks - 1 - step

        @pl.when(t != sp)
        def _():
            wait_recv(adj_in.at[t], r_adj.at[t])

        at = pl.ds(pl.multiple_of(t * BLOCK, BLOCK), BLOCK)
        gl = jnp.zeros((BLOCK, rank), F32)
        for i in range(rows):
            cols = slice(i * KW, (i + 1) * KW)
            b = bsum[t, :, cols]
            last = b[BLOCK - 1 : BLOCK, :]
            centre = b[middle : middle + 1, :]
            qs = q_ref[i, at, :].astype(F32) * scale
            kk = k_ref[i, at, :].astype(F32)
            vv = v_ref[i, at, :]
            do = adj_in[t, i]
            e_ql = jnp.exp(b - centre)
            e_kl = jnp.exp(centre - b)
            e_qh = jnp.exp(b)
            e_kh = jnp.exp(last - b)
            e_last = jnp.exp(last)
            ql = (qs * e_ql).astype(BF)
            kl = (kk * e_kl).astype(BF)
            qh = (qs * e_qh).astype(BF)
            kh = (kk * e_kh).astype(BF)
            ds = dstate[i]
            dsb = ds.astype(BF)
            st = states[t, i]
            a = jnp.where(causal, dot(ql, kl, NT), 0.0).astype(BF)
            da = jnp.where(causal, dot(do, vv, NT), 0.0).astype(BF)
            dql = dot(da, kl)
            dkl = dot(da, ql, TN)
            dqh = dot(do, st)
            dkh = dot(vv, dsb)
            gv = dot(a, do, TN) + dot(kh, dsb, NT)
            gq = (dql * e_ql + dqh * e_qh) * scale
            gk = dkl * e_kl + dkh * e_kh
            gbuf[t, i, :, 0:KW] = gq.astype(BF)
            gbuf[t, i, :, KW : 2 * KW] = gk.astype(BF)
            gbuf[t, i, :, 2 * KW : 2 * KW + VW] = gv.astype(BF)
            carried = jnp.sum(ds * st.astype(F32), axis=0, keepdims=True) * e_last
            dstate[i] = ds * e_last + dot(do, qh, TN)
            w1 = ql.astype(F32) * dql - kl.astype(F32) * dkl + qh.astype(F32) * dqh
            w2 = kh.astype(F32) * dkh
            gld = dot(grad_mat, jnp.concatenate(split(w1, 2) + split(w2, 2), axis=0)) + carried
            gp = (gld * slope[t, :, cols]).astype(BF)
            gpre[i, at, :] = gp
            gl += dot(gp, up_mine[:, cols], NT)
        glp[t] = gl

        @pl.when(t != sp)
        def _():
            gl_copy(t).start()
            g_copy(t).start()

        @pl.when(t == sp)
        def _():
            glp_in[t] = gl
            gqkv_ref[pl.ds(sp * rows, rows)] = gbuf[t]

    low_seq = low_all[:, pl.ds(pl.multiple_of(seq_of_me * BLOCK, BLOCK), BLOCK), :].reshape(
        blocks * BLOCK, rank
    )

    def ub_copy(i, j):
        return remote(
            ub.at[i, j], ub_in.at[dp * seqs + seq_of_me],
            s_ub.at[i, j], r_ub.at[dp * seqs + seq_of_me], j, head0 + i,
        )

    def ub_self(i, j):
        return jnp.logical_and(head0 + i == dp, sp == j)

    for i in range(rows):
        part = dot(low_seq, gpre[i], TN)
        bias = jnp.sum(gpre[i].astype(F32), axis=0, keepdims=True)
        for j in range(nj):
            ub[i, j, 0:8, :] = part[j * 8 : (j + 1) * 8, :]
            ub[i, j, 8:16, :] = jnp.broadcast_to(bias, (8, KW))
    for i in range(rows):
        for j in range(nj):

            @pl.when(jnp.logical_not(ub_self(i, j)))
            def _():
                ub_copy(i, j).start()

            @pl.when(ub_self(i, j))
            def _():
                ub_in[dp * seqs + seq_of_me] = ub[i, j]

    for s in range(n_sp):

        @pl.when(s != sp)
        def _():
            wait_recv(glp_in.at[s], r_gl.at[s])

    per_seq = n_sp // seqs
    glow = jnp.concatenate(
        [
            functools.reduce(
                lambda x, y: x + y, [glp_in[s] for s in range(b * per_seq, (b + 1) * per_seq)]
            )
            for b in range(seqs)
        ],
        axis=0,
    ).astype(BF)

    def gd_copy(i, j):
        return remote(
            gdp.at[i, j], gd_in.at[me], s_gd.at[i, j], r_gd.at[me], j, i
        )

    @pl.loop(0, n_dp)
    def _(d):
        i = lax.rem(dp + d, n_dp)
        gdp[i] = dot(glow, xp_ref[i], TN).reshape(nj, 8, xp_ref.shape[2])
        for j in range(nj):
            own = jnp.logical_and(i == dp, sp == j)

            @pl.when(jnp.logical_not(own))
            def _():
                gd_copy(i, j).start()

            @pl.when(own)
            def _():
                gd_in[me] = gdp[i, j]

    ub_owner = jnp.logical_and(dp < HEADS, sp < nj)

    @pl.when(ub_owner)
    def _():
        for b in range(seqs):
            holder = (b * HEADS + dp) // rows

            @pl.loop(0, n_dp)
            def _(d):
                @pl.when(jnp.logical_not(jnp.logical_and(d == dp, holder == sp)))
                def _():
                    wait_recv(ub_in.at[d * seqs + b], r_ub.at[d * seqs + b])

        ub_sum[...] = jnp.sum(ub_in[...], axis=0)
        gu_ref[dp, sp] = ub_sum[...]

        @pl.loop(1, n_all)
        def _(d):
            other = lax.rem(me + d, n_all)
            remote(
                ub_sum, gu_ref.at[dp, sp], s_us.at[d], r_us.at[dp, sp],
                lax.rem(other, n_sp), other // n_sp,
            ).start()

    @pl.loop(0, n_dp)
    def _(i):
        gi_ref[i] = dot(glow, down_all[i]).astype(BF)

    @pl.when(sp < nj)
    def _():
        @pl.loop(1, n_all)
        def _(d):
            other = lax.rem(me + d, n_all)
            wait_recv(gd_in.at[other], r_gd.at[other])

        gd_sum[...] = jnp.sum(gd_in[...], axis=0)
        gd_ref[sp] = gd_sum[...]
        for d in range(1, n_sp):
            remote(
                gd_sum, gd_ref.at[sp], s_gs.at[d], r_gs.at[sp], lax.rem(sp + d, n_sp), dp
            ).start()

    for j in range(nj):

        @pl.when(j != sp)
        def _():
            wait_recv(gd_ref.at[j], r_gs.at[j])

    @pl.loop(0, HEADS)
    def _(h):
        for j in range(nj):

            @pl.when(jnp.logical_not(jnp.logical_and(h == dp, j == sp)))
            def _():
                wait_recv(gu_ref.at[h, j], r_us.at[h, j])

    for s in range(n_sp):

        @pl.when(s != sp)
        def _():
            wait_recv(gqkv_ref.at[pl.ds(s * rows, rows)], r_g.at[s])

    def sent(src, sem):
        remote(src, src, sem, sem, sp, dp).wait_send()

    @pl.loop(1, n_dp)
    def _(d):
        sent(dt_ref, s_down.at[d])

    for d in range(1, n_sp):
        sent(adj_ref.at[pl.ds(0, rows)], s_adj.at[d])
        sent(low_all.at[sp], s_low.at[d])

    @pl.loop(0, blocks)
    def _(t):
        @pl.when(t != sp)
        def _():
            sent(gbuf.at[t], s_g.at[t])
            sent(glp.at[t], s_gl.at[t])

    for i in range(rows):
        for j in range(nj):

            @pl.when(jnp.logical_not(ub_self(i, j)))
            def _():
                sent(ub.at[i, j], s_ub.at[i, j])

    @pl.loop(0, n_dp)
    def _(i):
        for j in range(nj):

            @pl.when(jnp.logical_not(jnp.logical_and(i == dp, sp == j)))
            def _():
                sent(gdp.at[i, j], s_gd.at[i, j])

    @pl.when(ub_owner)
    def _():
        @pl.loop(1, n_all)
        def _(d):
            sent(ub_sum, s_us.at[d])

    @pl.when(sp < nj)
    def _():
        for d in range(1, n_sp):
            sent(gd_sum, s_gs.at[d])


def on_device(n_sp, n_dp, x, down, up, offs, q, k, v, extra, adj):
    seqs, local_len, width = x.shape
    rows, length, _ = q.shape
    piece, rank = down.shape
    wide = -(-piece // 128) * 128
    tokens = seqs * local_len
    nj = rank // 8
    n_all = n_sp * n_dp
    items = seqs * HEADS
    assert local_len == BLOCK and HEADS % rows == 0 and n_sp % seqs == 0
    assert n_dp >= HEADS and n_sp >= nj
    xp = jnp.pad(
        x.reshape(tokens, n_dp, piece).transpose(1, 0, 2), ((0, 0), (0, 0), (0, wide - piece))
    )
    dt = jnp.pad(down.T, ((0, 0), (0, wide - piece)))
    adj_items = (
        adj.reshape(seqs, local_len, HEADS, VW).transpose(0, 2, 1, 3).reshape(items, local_len, VW)
    )
    cat = 2 * KW + VW
    vm = pl.BlockSpec(memory_space=pltpu.VMEM)
    dma = pltpu.SemaphoreType.DMA
    gqkv, gi, gd, gu = pl.pallas_call(
        functools.partial(kernel, n_sp, n_dp, seqs, rows),
        out_shape=(
            jax.ShapeDtypeStruct((items, BLOCK, cat), BF),
            jax.ShapeDtypeStruct((n_dp, tokens, wide), BF),
            jax.ShapeDtypeStruct((nj, 8, wide), F32),
            jax.ShapeDtypeStruct((HEADS, nj, 16, KW), F32),
        ),
        in_specs=[vm] * 9,
        out_specs=(vm,) * 4,
        scratch_shapes=[
            pltpu.VMEM((n_dp, rank, wide), BF),
            pltpu.VMEM((n_sp, tokens, rank), BF),
            pltpu.VMEM((n_sp, rows, BLOCK, VW), BF),
            pltpu.VMEM((n_sp, rows, BLOCK, cat), BF),
            pltpu.VMEM((rows, VW, KW), F32),
            pltpu.VMEM((n_sp, rows, VW, KW), BF),
            pltpu.VMEM((rows, VW, KW), F32),
            pltpu.VMEM((n_sp, BLOCK, rows * KW), F32),
            pltpu.VMEM((n_sp, BLOCK, rows * KW), F32),
            pltpu.VMEM((rows, length, KW), BF),
            pltpu.VMEM((n_sp, BLOCK, rank), F32),
            pltpu.VMEM((n_sp, BLOCK, rank), F32),
            pltpu.VMEM((n_dp, nj, 8, wide), F32),
            pltpu.VMEM((n_all, 8, wide), F32),
            pltpu.VMEM((8, wide), F32),
            pltpu.VMEM((rows, nj, 16, KW), F32),
            pltpu.VMEM((n_dp * seqs, 16, KW), F32),
            pltpu.VMEM((16, KW), F32),
            dma((n_dp,)), dma((n_dp,)),
            dma((n_sp,)), dma((n_sp,)),
            dma((n_sp,)), dma((n_sp,)),
            dma((n_sp,)), dma((n_sp,)),
            dma((n_sp,)), dma((n_sp,)),
            dma((n_dp, nj)), dma((n_all,)),
            dma((n_sp,)), dma((nj,)),
            dma((rows, nj)), dma((n_dp * seqs,)),
            dma((n_all,)), dma((HEADS, nj)),
        ],
        compiler_params=pltpu.CompilerParams(
            collective_id=0, has_side_effects=True, vmem_limit_bytes=56 * 1024 * 1024
        ),
    )(xp, dt, up, offs.reshape(1, -1), q, k, v, extra.reshape(rows, length, 1), adj_items)

    g = gqkv.reshape(seqs, HEADS, local_len, cat).transpose(0, 2, 1, 3)
    gi = gi[:, :, :piece].transpose(1, 0, 2).reshape(seqs, local_len, width)
    gd = gd.reshape(rank, wide)[:, :piece].T
    up_grad = gu[:, :, :8].transpose(1, 2, 0, 3).reshape(rank, HEADS * KW)
    bias = gu[:, 0, 8].reshape(HEADS * KW)
    return (
        g[..., :KW].reshape(seqs, local_len, HEADS * KW),
        g[..., KW : 2 * KW].reshape(seqs, local_len, HEADS * KW),
        g[..., 2 * KW :].reshape(seqs, local_len, HEADS * VW),
        gi,
        gd,
        up_grad,
        bias,
    )


def solution(mesh):
    tok = P("dp", "sp", None)
    item = P(("dp", "sp"), None, None)
    return jax.shard_map(
        functools.partial(on_device, mesh.shape["sp"], mesh.shape["dp"]),
        mesh=mesh,
        in_specs=(tok, P("dp", None), P(), P(), item, item, item, P(("dp", "sp"), None), tok),
        out_specs=(tok, tok, tok, tok, P("dp", None), P(), P()),
        check_vma=False,
    )
```

time: 304 us -> 75 us (0.25); the launches traced: 300 us -> 74.5 us
  waiting for transfers between devices: 99.7 us -> 0 us
  blocking collectives: 62.2 us -> 0 us
  Pallas kernels: 0 us -> 57.6 us
  starting transfers between devices: 35.4 us -> 0 us
  matrix products: 30 us -> 0 us
  other arithmetic: 21.5 us -> 0 us
  local copies, waits for them, and re-layouts: 36.1 us -> 16.2 us
  between operations: 14.3 us -> 0.72 us
    psum x1 -> x0, waiting for transfers between devices: 93.1 us -> none  [on_device(): lax.psum((whole_term, up_term, bias_term), ('sp', 'dp'))]
    pallas_call x0 -> x1, Pallas kernels: none -> 57.6 us  [on_device(): pl.pallas_call(functools.partial(kernel, n_sp, n_dp, seqs, rows), out_sha...]
    psum x1 -> x0, blocking collectives: 40 us -> none  [on_device(): lax.psum((whole_term, up_term, bias_term), ('sp', 'dp'))]
    all_to_all x6 -> x0, starting transfers between devices: 35.4 us -> none  [the longest x1 10.3 us: on_device(): lax.all_to_all(pre_items, 'sp', split_axis=0, concat_axis=1, tiled=True)]
    dot_general x46 -> x0, matrix products: 30 us -> none  [the longest x12 11 us: advance(): jnp.dot(fading.T, value_block, precision=highest)]
    all_gather x1 -> x0, blocking collectives: 22.2 us -> none  [on_device(): lax.all_gather(forgetting_narrowing_matrix, 'dp', axis=0, tiled=True)]
    squeeze x20 -> x0, local copies, waits for them, and re-layouts: 13.2 us -> none  [head_forward(): lax.scan(jax.checkpoint(advance), initial, (blocked(scaled), blocked(stre...]
    another operation x6 -> x0, other arithmetic: 7.06 us -> none  [the longest x2 6.91 us: head_forward(): decay_sums = jnp.cumsum(blocked(retention_coefficient), axis=1)]
  transfers between devices with their start and end apart: 7 -> 0, of which waited for: 3 -> 0; matrix products, arithmetic and copies ran while one was open for 10% -> 0% of each run, Pallas kernels for 0% -> 0%
where the time goes in v1:
time: 75 us; the launch traced here: 74.5 us
  Pallas kernels  57.6 us (77%)
  local copies, waits for them, and re-layouts  16.2 us (22%)
    pallas_call x1, Pallas kernels, on_device(): pl.pallas_call(functools.partial(kernel, n_sp, n_dp, seqs, rows), out_sha...  57.6 us
    unnamed x11, local copies, waits for them, and re-layouts  2.75 us
    reshape x1, local copies, waits for them, and re-layouts, on_device(): extra.reshape(rows, length, 1)  1.71 us

profile of v1, /device:TPU:29, one launch (start us, length us, event | category | flops | bytes accessed | tf_op | source)
XLA Modules:
  0.0 74.5 jit_solution(16255914135769595218)
XLA Ops:
  0.6 0.0 copy-start.3
  0.6 1.4 %pad.9.dt_ref = bf16[32,384]{1,0:T(8,128)(2,1)} pad(bf16[32,258]{1,0:T(8,128)(2,1)} %bitcast.50, bf16[]{:T(256)} %constant.2.clone.1), padding=0_0x0_126 | pad | bytes 41090 | tf_op jit(solution)/shard_map/jit(_pad)/pad | solution.py:417
  2.1 1.7 %copy.22.extra_ref = f32[4,256,1]{2,1,0:T(8,128)} copy(f32[4,256,1]{1,0,2:T(4,128)} %bitcast.51) | data formatting | bytes 8192 | tf_op jit(solution)/shard_map/reshape | solution.py:466
  3.8 0.0 copy-done.3
  3.8 0.0 copy-start.2
  3.8 0.8 %copy.40 = bf16[2,8,8,8,256]{4,3,1,2,0:T(8,128)(2,1)} copy(bf16[2,8,8,8,256]{4,3,2,1,0:T(8,128)(2,1)S(1)} %bitcast.46) | data formatting | bytes 1048576 | tf_op jit(solution)/shard_map/reshape | solution.py:419
  4.6 0.4 copy-done.2
  5.0 0.9 %reshape.50 = bf16[128,8,258]{2,1,0:T(8,128)(2,1)S(1)} reshape(bf16[2,64,2064]{2,1,0:T(8,128)(2,1)S(1)} %copy-done.2) | data formatting | bytes 1056768 | tf_op jit(solution)/shard_map/reshape | solution.py:415
  5.9 0.1 copy.39
  6.0 1.0 %pad.8.xp_ref = bf16[8,128,384]{2,1,0:T(8,128)(2,1)} pad(bf16[8,128,258]{2,1,0:T(8,128)(2,1)S(1)} %bitcast.42, bf16[]{:T(256)} %constant.2.clone.1), padding=0_0x0_0x0_126 | pad | bytes 1314818 | tf_op jit(solution)/shard_map/jit(_pad)/pad | solution.py:414
  7.0 57.6 %shard_map.144 = (bf16[16,64,512]{2,1,0:T(8,128)(2,1)}, bf16[8,128,384]{2,1,0:T(8,128)(2,1)}, f32[4,8,384]{2,1,0:T(8,128)}, f32[8,4,16,128]{3,2,1,0:T(8,128)}) custom-call(bf16[8,128,384]{2,1,0:T(8,128)(2,1)} %pad.8.xp_ref, bf16[32,384]{1,0:T(8,128)(2,1)} %pad.9.dt_ref, bf16[32,1024]{1,0:T(8,128)(2,1)} %up_ref.1, f32[1,1024]{1,0:T(1,128)} %bitcast.52, ...), custom_call_target="tpu_custom_call" | custom-call | tf_op jit(solution)/shard_map/pallas_call | solution.py:424
  64.6 0.0 copy-start
  64.6 1.4 %slice.27 = f32[8,1,1,128]{3,2,1,0:T(1,128)} slice(f32[8,4,16,128]{3,2,1,0:T(8,128)} %get-tuple-element.14), slice={[0:8], [0:1], [8:9], [0:128]} | slice | bytes 8192 | tf_op jit(solution)/shard_map/slice | solution.py:472
  66.1 0.9 %slice_bitcast_fusion.4 = f32[4,8,8,128]{3,1,0,2:T(8,128)S(1)} fusion(f32[8,4,16,128]{3,2,1,0:T(8,128)} %get-tuple-element.14), kind=kLoop, calls=%fused_computation.10 | loop fusion | bytes 262144 | tf_op jit(solution)/shard_map/transpose | solution.py:471
  67.0 0.1 copy.42
  67.1 0.7 copy.41
  67.8 1.4 %slice_bitcast_fusion.5 = f32[258,32]{0,1:T(8,128)} fusion(f32[32,384]{1,0:T(8,128)} %bitcast.49), kind=kLoop, calls=%fused_computation.11 | loop fusion | bytes 66048 | tf_op jit(solution)/shard_map/transpose | solution.py:470
  69.2 1.1 %slice_bitcast_fusion.1 = bf16[2,8,8,8,256]{4,3,2,1,0:T(8,128)(2,1)S(1)} fusion(bf16[2,64,8,512]{3,1,2,0:T(8,128)(2,1)} %bitcast.44), kind=kLoop, calls=%fused_computation.3 | loop fusion | bytes 1048576
  70.3 0.0 copy-done
  70.3 0.1 slice_bitcast_fusion.2
  70.4 0.8 %copy.31 = bf16[2,8,8,8,256]{4,3,1,2,0:T(8,128)(2,1)} copy(bf16[2,8,8,8,256]{4,3,2,1,0:T(8,128)(2,1)S(1)} %slice_bitcast_fusion.1) | data formatting | bytes 1048576 | tf_op jit(solution)/shard_map/reshape | solution.py:476
  71.3 0.0 copy-start.1
  71.3 0.9 %copy_bitcast_fusion.2 = (bf16[2,64,1024]{2,1,0:T(8,128)(2,1)}, bf16[2,64,1024]{2,1,0:T(8,128)(2,1)}) fusion(bf16[2,8,8,8,128]{4,3,2,1,0:T(8,128)(2,1)S(1)} %get-tuple-element.15, bf16[2,8,8,8,128]{4,3,2,1,0:T(8,128)(2,1)S(1)} %get-tuple-element.16), kind=kLoop, calls=%fused_computation.4 | loop fusion | bytes 1048576 | tf_op jit(solution)/shard_map/reshape | solution.py:475
  72.2 0.4 copy-done.1
  72.6 0.1 slice_bitcast_fusion
  72.7 0.5 copy.26
  73.1 1.4 %reshape.59 = bf16[2,64,2064]{2,1,0:T(8,128)(2,1)} reshape(bf16[128,8,258]{2,1,0:T(8,128)(2,1)S(1)} %copy.26) | data formatting | bytes 1056768 | tf_op jit(solution)/shard_map/reshape | solution.py:469
Async XLA Ops:
  0.6 3.1 %copy-start.3 = (bf16[2,64,2048]{2,1,0:T(8,128)(2,1)S(1)}, bf16[2,64,2048]{2,1,0:T(8,128)(2,1)}, u32[]{:S(2)}) copy-start(bf16[2,64,2048]{2,1,0:T(8,128)(2,1)} %param.17) | copy-start | bytes 1572868
  3.8 1.2 %copy-start.2 = (bf16[2,64,2064]{2,1,0:T(8,128)(2,1)S(1)}, bf16[2,64,2064]{2,1,0:T(8,128)(2,1)}, u32[]{:S(2)}) copy-start(bf16[2,64,2064]{2,1,0:T(8,128)(2,1)} %param.9) | copy-start | bytes 1585156
  64.6 5.6 %copy-start = (bf16[16,64,512]{2,1,0:T(8,128)(2,1)S(1)}, bf16[16,64,512]{2,1,0:T(8,128)(2,1)}, u32[]{:S(2)}) copy-start(bf16[16,64,512]{2,1,0:T(8,128)(2,1)} %get-tuple-element.11) | copy-start | bytes 3145732
  71.3 1.3 %copy-start.1 = (bf16[8,128,384]{2,1,0:T(8,128)(2,1)S(1)}, bf16[8,128,384]{2,1,0:T(8,128)(2,1)}, u32[]{:S(2)}) copy-start(bf16[8,128,384]{2,1,0:T(8,128)(2,1)} %get-tuple-element.12) | copy-start | bytes 2359300
